TPU v7x, 512 devices: a whole 4x8x8 slice. The times are simulated.
512 devices in a mesh: sp: 64 (over z, y), tp: 8 (over x, core).
Axes of the slice: x: 4, y: 8, z: 8, core: 2. Of those that a mesh axis runs over, the one named last changes fastest.
Arguments:
- value_in: bfloat16 [23040, 2048], P('sp', 'tp'), may hold values from -240 to 240
- gate_in: bfloat16 [23040, 2048], P('sp', 'tp'), may hold values from -8 to 8
- taps: float32 [31, 2048], P(None, 'tp'), may hold values from -1 to 1
- norm_gain: float32 [2048], P('tp'), may hold values from 0.1 to 1.9
- norm_bias: float32 [2048], P('tp'), may hold values from -3 to 3
- proj_weight: bfloat16 [2048, 4096], P('tp', 'sp'), may hold values from -0.125 to 0.125
- out_grad: bfloat16 [23040, 4096], P('sp'), may hold values from -16 to 16
Outputs:
- value_grad: bfloat16 [23040, 2048], P('sp', 'tp')
- gate_grad: bfloat16 [23040, 2048], P('sp', 'tp')
- tap_grad: float32 [31, 2048], P(None, 'tp')
- gain_grad: float32 [2048], P('tp')
- bias_grad: float32 [2048], P('tp')
- weight_grad: float32 [2048, 4096], P('tp', 'sp')
All inputs are finite; a program needn't handle non-finite values.
Results may differ from a plain program's by a relative error of at most 0.0051.
Values may be sent and summed in bfloat16 or wider, within the bound.
A program may use at most 64 MiB of HBM per device.

v0:
```python
import functools
import jax
import jax.numpy as jnp
from jax import lax
from jax.sharding import Mesh
from jax.sharding import PartitionSpec as P

SP = ("sp_0", "sp_1")


def padded_2(cells, sides, width):
    for axis, dim in sides:
        count = lax.axis_size(axis)
        ends = count - 1
        head = lax.slice_in_dim(cells, 0, width, axis=dim)
        tail = lax.slice_in_dim(cells, cells.shape[dim] - width, cells.shape[dim], axis=dim)
        cells = jnp.concatenate(
            [
                lax.ppermute(tail, axis, [(i, (i + 1) % count) for i in range(ends)]),
                cells,
                lax.ppermute(head, axis, [((i + 1) % count, i) for i in range(ends)]),
            ],
            axis=dim,
        )
    return cells


def copy_for_each(value, axis):
    copies = jnp.broadcast_to(value, (lax.axis_size(axis), *value.shape))
    return lax.all_to_all(copies, axis, split_axis=0, concat_axis=0, tiled=True)


def of_everyone(value, axis):
    everything = copy_for_each(value, axis)
    return jnp.sum(everything, axis=0)


def together(arrays, axis):
    flat, at, finished = (jnp.concatenate([a.reshape(-1) for a in arrays]), 0, [])
    subtotal = of_everyone(flat, axis)
    for a in arrays:
        finished.append(subtotal[at : at + a.size].reshape(a.shape))
        at += a.size
    return tuple(finished)


def in_order(tiles, dim):
    tiles = jnp.moveaxis(tiles, 0, dim)
    lengths = tiles.shape
    return tiles.reshape(*lengths[:dim], lengths[dim] * lengths[dim + 1], *lengths[dim + 2 :])


def stacked_from(value, axes, order):
    tiles = value[None]
    for k in order:
        tiles = lax.all_gather(tiles, axes[k], axis=0, tiled=True)
    held = [lax.axis_size(axes[k]) for k in reversed(order)]
    tiles = tiles.reshape(*held, *value.shape)
    turned = sorted(range(len(order)), key=lambda place: order[len(order) - 1 - place])
    return tiles.transpose(*turned, *range(len(order), tiles.ndim)).reshape(-1, *value.shape)


def gather_axes(value, axes, order, dim):
    return in_order(stacked_from(value, axes, order), dim)


def passed_along(block, axis, distance):
    devices = range(lax.axis_size(axis))
    route = [(i - distance, i) for i in devices if i - distance in devices]
    return lax.ppermute(block, axis, route)


def by_axis(value, axes):
    return functools.reduce(lax.psum, axes, value)


def summed_rows(subtotal, axes):
    for axis in axes:
        subtotal = lax.psum_scatter(subtotal, axis, scatter_dimension=0, tiled=True)
    return subtotal


def on_device(value_in, gate_in, taps, norm_gain, norm_bias, proj_weight, out_grad):
    f32 = jnp.float32
    rows = value_in.shape[0]
    local_width = value_in.shape[1]
    span = taps.shape[0]
    half = span // 2
    width_all = local_width * lax.axis_size("tp")
    gate_sig = jax.nn.sigmoid(gate_in.astype(f32))
    value_f = value_in.astype(f32)
    mixed = (value_f * gate_sig).astype(jnp.bfloat16)
    padded = padded_2(mixed, ((SP, 0),), half).astype(f32)
    conv = jnp.zeros((rows, local_width), f32)
    for k in range(span):
        conv = conv + taps[k] * padded[k : k + rows]
    total, squares = together((jnp.sum(conv, axis=1), jnp.sum(conv * conv, axis=1)), "tp")
    mean = total / width_all
    centred = conv - mean[:, None]
    spread = squares / width_all - mean * mean
    inv = lax.rsqrt(spread + 1e-06)
    normed = centred * inv[:, None]
    pre = normed * norm_gain + norm_bias
    act = jax.nn.silu(pre).astype(jnp.bfloat16)
    columns = out_grad
    act_grad = lax.dot_general(
        columns,
        gather_axes(proj_weight, SP, (0, 1), 1),
        (((1,), (1,)), ((), ())),
        preferred_element_type=f32,
    )
    sig_pre = jax.nn.sigmoid(pre)
    pre_grad = act_grad * sig_pre * (1.0 + pre * (1.0 - sig_pre))
    normed_grad = pre_grad * norm_gain
    first, second = together(
        (jnp.sum(normed_grad, axis=1), jnp.sum(normed_grad * normed, axis=1)), "tp"
    )
    conv_grad = inv[:, None] * (
        normed_grad - first[:, None] / width_all - normed * second[:, None] / width_all
    )
    local_pad = jnp.pad(conv_grad, ((2 * half, 2 * half), (0, 0)))
    spread_out = jnp.zeros((rows + 2 * half, local_width), f32)
    for k in range(span):
        spread_out = spread_out + taps[k] * local_pad[2 * half - k : 2 * half - k + rows + 2 * half]
    own_part = spread_out[half : half + rows]
    from_left = passed_along(spread_out[rows + half :], SP, 1)
    from_right = passed_along(spread_out[:half], SP, -1)
    mixed_grad = own_part.at[:half].add(from_left).at[rows - half :].add(from_right)
    tap_local = jnp.stack([jnp.sum(conv_grad * padded[k : k + rows], axis=0) for k in range(span)])
    gain_local = jnp.sum(pre_grad * normed, axis=0)
    bias_local = jnp.sum(pre_grad, axis=0)
    tap_grad, gain_grad, bias_grad = (
        by_axis(tap_local, SP),
        by_axis(gain_local, SP),
        by_axis(bias_local, SP),
    )
    value_grad = (mixed_grad * gate_sig).astype(jnp.bfloat16)
    gate_grad = (mixed_grad * value_f * gate_sig * (1.0 - gate_sig)).astype(jnp.bfloat16)
    columns = out_grad
    summed = summed_rows(
        lax.dot_general(columns, act, (((0,), (0,)), ((), ())), preferred_element_type=f32), SP
    )
    weight_grad = jnp.transpose(summed)
    return (value_grad, gate_grad, tap_grad, gain_grad, bias_grad, weight_grad)


def solution(mesh):
    finer = Mesh(mesh.devices.reshape(8, 8, mesh.shape["tp"]), ("sp_0", "sp_1", "tp"))
    in_specs = (P(SP, "tp"), P(SP, "tp"), P(None, "tp"), P("tp"), P("tp"), P("tp", SP), P(SP, None))
    out_specs = (P(SP, "tp"), P(SP, "tp"), P(None, "tp"), P("tp"), P("tp"), P("tp", SP))
    return jax.shard_map(
        on_device, mesh=finer, in_specs=in_specs, out_specs=out_specs, check_vma=False
    )
```

profile of v0, /device:TPU:4, one launch (start us, length us, event | category | flops | bytes accessed | tf_op | source)
XLA Modules:
  0.0 201.0 jit_solution(267206037773052146)
XLA Ops:
  8.1 31.5 %all-gather = bf16[2048,64]{0,1:T(8,128)(2,1)S(1)} all-gather(bf16[256,64]{0,1:T(8,128)(2,1)} %param.16), channel_id=2, replica_groups=mesh['sp_0'=8,'sp_1'=8,'tp'=8] {'sp_0'}, dimensions={0}, use_global_device_ids=true | all-gather | bytes 294912 | tf_op jit(solution)/shard_map/all_gather | solution.py:56
  40.4 1.1 fusion.62
  41.5 3.5 %collective-permute-start = (bf16[15,256]{1,0:T(8,128)(2,1)S(1)}, bf16[15,256]{1,0:T(8,128)(2,1)S(1)}, u32[]{:S(2)}, u32[]{:S(2)}) collective-permute-start(bf16[15,256]{1,0:T(8,128)(2,1)S(1)} %get-tuple-element.121), channel_id=1, source_target_pairs={{0,8},{8,16},{16,24},{24,32},{32,40},{40,48},{48,56},{56,64},{64,7... | collective-permute-start | bytes 23048 | tf_op jit(solution)/shard_map/ppermute | solution.py:19
  45.0 1.3 collective-permute-start.1
  46.3 1.0 fusion.75
  48.3 2.2 %collective-permute-done.1 = bf16[15,256]{1,0:T(8,128)(2,1)S(1)} collective-permute-done((bf16[15,256]{1,0:T(8,128)(2,1)S(1)}, bf16[15,256]{1,0:T(8,128)(2,1)S(1)}, u32[]{:S(2)}, u32[]{:S(2)}) %collective-permute-start.1) | collective-permute-done | bytes 7712 | tf_op jit(solution)/shard_map/ppermute | solution.py:21
  50.6 2.2 %fusion.72 = (f32[360]{0:T(512)S(1)}, f32[360]{0:T(512)S(1)}, f32[360,256]{1,0:T(8,128)}) fusion(f32[390,256]{1,0:T(8,128)S(1)} %maximum_convert_fusion, f32[256]{0:T(256)S(1)} %bitcast.144, f32[256]{0:T(256)S(1)} %bitcast.146, f32[256]{0:T(256)S(1)} %bitcast.88, f32[256]{0:T(256)S(1)} %bitcast.90, f32[256]{0:T(256)S(1)} %bitcast.92, f32[256]{0:T(256)S(1)} %bitcast.94, ...), kind=kLoop, calls=%fused_computation.158 | loop fusion | flops 5897520 | bytes 11831104 | tf_op jit(solution)/shard_map/reduce_sum | solution.py:97
  52.9 7.6 %all_to_all.12 = f32[8,1,720]{2,1,0:T(1,128)S(1)} all-to-all(f32[8,1,720]{2,1,0:T(1,128)S(1)} %broadcast_in_dim.6), channel_id=1, replica_groups=mesh['sp_0'=8,'sp_1'=8,'tp'=8] {'tp'}, dimensions={0} | all-to-all | bytes 46080 | tf_op jit(solution)/shard_map/all_to_all | solution.py:30
  60.6 4.4 %convolution_bitcast_fusion = f32[4096,256]{0,1:T(8,128)} fusion(bf16[360,4096]{1,0:T(8,128)(2,1)S(1)} %copy-done, f32[360,256]{1,0:T(8,128)} %get-tuple-element.116, f32[256]{0:T(256)S(1)} %copy-done.6, f32[256]{0:T(256)S(1)} %copy-done.5, f32[360]{0:T(512)S(1)} %get-tuple-element.157, f32[360]{0:T(512)S(1)} %get-tuple-element.156), kind=kOutput, calls=%fused_computation | convolution fusion | flops 755804160 | bytes 7516992 | tf_op jit(solution)/shard_map/dot_general | solution.py:141
  65.1 24.0 %all-gather.3.cloned.1.call-done = bf16[64,256,64]{1,0,2:T(8,128)(2,1)} async-done(((bf16[8,256,64]{1,0,2:T(8,128)(2,1)}), bf16[64,256,64]{1,0,2:T(8,128)(2,1)}) %all-gather.3.cloned.1.call-update) | async-done | bytes 2097168 | tf_op jit(solution)/shard_map/all_gather | solution.py:56
  89.0 2.8 %copy.28 = bf16[8,8,256,64]{2,3,1,0:T(8,128)(2,1)S(1)} copy(bf16[8,8,256,64]{2,0,1,3:T(8,128)(2,1)} %bitcast.82) | data formatting | bytes 4194304 | tf_op jit(solution)/shard_map/transpose | solution.py:60
  91.9 2.4 %multiply_reduce_fusion = (f32[256]{0:T(256)}, f32[360]{0:T(512)S(1)}, f32[360]{0:T(512)S(1)}, f32[256]{0:T(256)}, f32[360,256]{1,0:T(8,128)}) fusion(f32[360,256]{1,0:T(8,128)S(1)} %copy-done.1, f32[360]{0:T(512)S(1)} %get-tuple-element.157, f32[360]{0:T(512)S(1)} %get-tuple-element.156, f32[256]{0:T(256)S(1)} %copy-done.5, f32[256]{0:T(256)S(1)} %copy-done.6, ...), kind=kOutput, calls=%fused_computation.102 | convolution fusion | flops 756724480 | bytes 5793408 | tf_op jit(solution)/shard_map/dot_general | solution.py:106
  94.4 7.6 %all_to_all.13 = f32[8,1,720]{2,1,0:T(1,128)S(1)} all-to-all(f32[8,1,720]{2,1,0:T(1,128)S(1)} %broadcast_in_dim.8), channel_id=1, replica_groups=mesh['sp_0'=8,'sp_1'=8,'tp'=8] {'tp'}, dimensions={0} | all-to-all | bytes 46080 | tf_op jit(solution)/shard_map/all_to_all | solution.py:30
  102.0 2.6 %multiply_reduce_fusion.1 = (f32[256]{0:T(256)S(1)}, f32[256]{0:T(256)}, f32[256]{0:T(256)}, f32[256]{0:T(256)}, f32[256]{0:T(256)}, /*index=5*/f32[256]{0:T(256...) fusion(f32[390,256]{1,0:T(8,128)S(1)} %maximum_convert_fusion, ...), kind=kLoop, calls=%fused_computation.103 | loop fusion | flops 4050432 | bytes 7766656 | tf_op jit(solution)/shard_map/reduce_sum | solution.py:129
  105.3 1.2 fusion.55
  107.9 1.3 collective-permute-start.3
  109.2 5.1 %collective-permute-start.2 = (f32[15,256]{1,0:T(8,128)}, f32[15,256]{1,0:T(8,128)}, u32[]{:S(2)}, u32[]{:S(2)}) collective-permute-start(f32[15,256]{1,0:T(8,128)} %get-tuple-element.120), channel_id=1, source_target_pairs={{0,8},{8,16},{16,24},{24,32},{32,40},{40,48},{48,56},{56,64},{64,7... | collective-permute-start | bytes 46088 | tf_op jit(solution)/shard_map/ppermute | solution.py:70
  114.4 8.1 %reduce-scatter.5.cloned.1.call-done = f32[512,256]{0,1:T(8,128)} async-done(((f32[4096,256]{0,1:T(8,128)}), f32[512,256]{0,1:T(8,128)}) %reduce-scatter.5.cloned.1.call-update) | async-done | bytes 524304 | tf_op jit(solution)/shard_map/reduce_scatter | solution.py:79
  122.4 2.0 %copy.32 = f32[512,256]{1,0:T(8,128)} copy(f32[512,256]{0,1:T(8,128)} %reduce-scatter.5.cloned.1.call-done) | data formatting | bytes 1048576
  124.5 2.2 %multiply_reduce_fusion.19 = (f32[256]{0:T(256)}, f32[256]{0:T(256)}, f32[256]{0:T(256)}, f32[256]{0:T(256)}, f32[256]{0:T(256)}, /*index=5*/f32[256]{0:T(256)},...) fusion(f32[360,256]{1,0:T(8,128)} %copy-done.2, ...), kind=kLoop, calls=%fused_computation.121 | loop fusion | flops 2392832 | bytes 5174272 | tf_op jit(solution)/shard_map/reduce_sum | solution.py:129
  126.7 2.9 %stack.127 = f32[31,256]{1,0:T(8,128)S(1)} concatenate(f32[1,256]{1,0:T(1,128)} %bitcast.178, f32[1,256]{1,0:T(1,128)} %bitcast.177, f32[1,256]{1,0:T(1,128)} %bitcast.176, f32[1,256]{1,0:T(1,128)} %bitcast.175, f32[1,256]{1,0:T(1,128)} %bitcast.174, f32[1,256]{1,0:T(1,128)} %bitcast.173, f32[1,256]{1,0:T(1,128)} %bitcast.172, f32[1,256]{1,0:T(1,128)} %bitcast.171, ...), dimensions={0} | concatenate | bytes 63488 | tf_op jit(solution)/shard_map/stack | solution.py:129
  129.5 29.3 %all-reduce.2 = (f32[31,256]{1,0:T(8,128)S(1)}, f32[256]{0:T(256)S(1)}, f32[256]{0:T(256)S(1)}) all-reduce(f32[31,256]{1,0:T(8,128)S(1)} %stack.127, f32[256]{0:T(256)} %get-tuple-element.103, f32[256]{0:T(256)} %get-tuple-element.106), channel_id=1, replica_groups=mesh['sp_0'=8,'sp_1'=8,'tp'=8] {'sp_0'}, use_global_device_ids=true, to_apply=%region_37.38 | all-reduce | flops 8448 | bytes 67584 | tf_op jit(solution)/shard_map/psum | solution.py:74
  158.8 30.7 %all-reduce.1 = (f32[31,256]{1,0:T(8,128)}, f32[256]{0:T(256)}, f32[256]{0:T(256)}) all-reduce(f32[31,256]{1,0:T(8,128)S(1)} %get-tuple-element.112, f32[256]{0:T(256)S(1)} %get-tuple-element.113, f32[256]{0:T(256)S(1)} %get-tuple-element.114), channel_id=1, replica_groups=mesh['sp_0'=8,'sp_1'=8,'tp'=8] {'sp_1'}, use_global_device_ids=true, to_apply=%region_38.39 | all-reduce | flops 8448 | bytes 67584 | tf_op jit(solution)/shard_map/psum | solution.py:74
  191.7 1.8 fusion.65
  (42 shorter events, 6.7 us)
Async XLA Ops:
  8.0 52.6 %copy-start = (bf16[360,4096]{1,0:T(8,128)(2,1)S(1)}, bf16[360,4096]{1,0:T(8,128)(2,1)}, u32[]{:S(2)}) copy-start(bf16[360,4096]{1,0:T(8,128)(2,1)} %param.17) | copy-start | bytes 8847364
  8.0 81.0 %all-gather.3.cloned.1.call-start = ((), (), s32[]{:S(2)}) async-start(), calls=%async_computation.4 | async-start | bytes 2359296 | tf_op jit(solution)/shard_map/all_gather | solution.py:56
  40.3 82.1 %reduce-scatter.5.cloned.1.call-start = ((), (), s32[]{:S(2)}) async-start(), calls=%async_computation.5 | async-start | bytes 4718592 | tf_op jit(solution)/shard_map/reduce_scatter | solution.py:79
  41.5 6.8 %collective-permute-start = (bf16[15,256]{1,0:T(8,128)(2,1)S(1)}, bf16[15,256]{1,0:T(8,128)(2,1)S(1)}, u32[]{:S(2)}, u32[]{:S(2)}) collective-permute-start(bf16[15,256]{1,0:T(8,128)(2,1)S(1)} %get-tuple-element.121), channel_id=1, source_target_pairs={{0,8},{8,16},{16,24},{24,32},{32,40},{40,48},{48,56},{56,64},{64,7... | collective-permute-start | bytes 23048 | tf_op jit(solution)/shard_map/ppermute | solution.py:19
  45.0 5.5 %collective-permute-start.1 = (bf16[15,256]{1,0:T(8,128)(2,1)S(1)}, bf16[15,256]{1,0:T(8,128)(2,1)S(1)}, u32[]{:S(2)}, u32[]{:S(2)}) collective-permute-start(bf16[15,256]{1,0:T(8,128)(2,1)S(1)} %get-tuple-element.122), channel_id=1, source_target_pairs={{8,0},{16,8},{24,16},{32,24},{40,32},{48,40},{56,48},{64,56},{72,6... | collective-permute-start | bytes 23048 | tf_op jit(solution)/shard_map/ppermute | solution.py:21
  50.6 10.0 %copy-start.5 = (f32[256]{0:T(256)S(1)}, f32[256]{0:T(256)}, u32[]{:S(2)}) copy-start(f32[256]{0:T(256)} %param.14) | copy-start | bytes 3076
  50.6 10.0 %copy-start.6 = (f32[256]{0:T(256)S(1)}, f32[256]{0:T(256)}, u32[]{:S(2)}) copy-start(f32[256]{0:T(256)} %param.15) | copy-start | bytes 3076
  65.0 128.5 %reduce-scatter.7.cloned.1.call-start = ((), (), s32[]{:S(2)}) async-start(), calls=%async_computation.6 | async-start | bytes 589824
  89.0 2.8 %copy-start.1 = (f32[360,256]{1,0:T(8,128)S(1)}, f32[360,256]{1,0:T(8,128)}, u32[]{:S(2)}) copy-start(f32[360,256]{1,0:T(8,128)} %get-tuple-element.116) | copy-start | bytes 1105924
  104.6 0.7 copy-start.2
  106.6 0.8 copy-start.3
  107.9 83.6 %collective-permute-start.3 = (f32[15,256]{1,0:T(8,128)}, f32[15,256]{1,0:T(8,128)S(1)}, u32[]{:S(2)}, u32[]{:S(2)}) collective-permute-start(f32[15,256]{1,0:T(8,128)} %get-tuple-element.119), channel_id=1, source_target_pairs={{8,0},{16,8},{24,16},{32,24},{40,32},{48,40},{56,48},{64,56},{72,6... | collective-permute-start | bytes 46088 | tf_op jit(solution)/shard_map/ppermute | solution.py:70
  109.2 81.3 %collective-permute-start.2 = (f32[15,256]{1,0:T(8,128)}, f32[15,256]{1,0:T(8,128)}, u32[]{:S(2)}, u32[]{:S(2)}) collective-permute-start(f32[15,256]{1,0:T(8,128)} %get-tuple-element.120), channel_id=1, source_target_pairs={{0,8},{8,16},{16,24},{24,32},{32,40},{40,48},{48,56},{56,64},{64,7... | collective-permute-start | bytes 46088 | tf_op jit(solution)/shard_map/ppermute | solution.py:70
  124.5 67.2 %copy-start.4 = (bf16[360,256]{1,0:T(8,128)(2,1)S(1)}, bf16[360,256]{1,0:T(8,128)(2,1)}, u32[]{:S(2)}) copy-start(bf16[360,256]{1,0:T(8,128)(2,1)} %param.11) | copy-start | bytes 552964
Sparse Core Ops, SparseCore 0:
  40.5 48.5 all-gather.2
  124.6 38.2 reduce-scatter.6
Sparse Core Ops, SparseCore 1:
  65.1 57.3 reduce-scatter.4
where the time goes:
time: 202 us; the launch traced here: 201 us
  blocking collectives  107 us (53%)
  waiting for transfers between devices  34.3 us (17%)
  between operations  15.7 us (8%)
  local copies, waits for them, and re-layouts  14.1 us (7%)
  other arithmetic  12.2 us (6%)
  starting transfers between devices  11.3 us (6%)
  matrix products  6.77 us (3%)
    psum x2, blocking collectives, by_axis(): return functools.reduce(lax.psum, axes, value)  59.9 us
    all_gather x1, blocking collectives, stacked_from(): tiles = lax.all_gather(tiles, axes[k], axis=0, tiled=True)  31.5 us
    all_gather x1, waiting for transfers between devices, stacked_from(): tiles = lax.all_gather(tiles, axes[k], axis=0, tiled=True)  24 us
    all_to_all x2, blocking collectives, copy_for_each(): return lax.all_to_all(copies, axis, split_axis=0, concat_axis=0, tiled=True)  15.2 us
    reduce_scatter x1, waiting for transfers between devices, summed_rows(): subtotal = lax.psum_scatter(subtotal, axis, scatter_dimension=0, tiled=True)  8.09 us
    ppermute x2, starting transfers between devices, passed_along(): return lax.ppermute(block, axis, route)  6.43 us
    reduce_sum x2, other arithmetic, on_device(): jnp.sum(conv_grad * padded[k:k + rows], axis=0)  4.71 us
    dot_general x1, matrix products, on_device(): lax.dot_general(columns, act, (((0,), (0,)), ((), ())), preferred_element...  4.37 us
  transfers between devices with their start and end apart: 7, of which 3 were waited for; matrix products, arithmetic and copies ran while one was open for 15% of the time, Pallas kernels for 0%

commit v1 on v0

--- a/solution.py
+++ b/solution.py
@@ -53,7 +53,9 @@
 def stacked_from(value, axes, order):
     tiles = value[None]
     for k in order:
-        tiles = lax.all_gather(tiles, axes[k], axis=0, tiled=True)
+        tiles = jnp.concatenate(
+            lax.all_to_all(jnp.stack([tiles] * lax.axis_size(axes[k])), axes[k], 0, 0), axis=0
+        )
     held = [lax.axis_size(axes[k]) for k in reversed(order)]
     tiles = tiles.reshape(*held, *value.shape)
     turned = sorted(range(len(order)), key=lambda place: order[len(order) - 1 - place])

time: 202 us -> 213 us (1.054)
  the two profiles are of different devices: /device:TPU:4 before, /device:TPU:2 now
where the time goes in v1:
time: 213 us; the launch traced here: 212 us
  blocking collectives  152 us (71%)
  between operations  14.2 us (7%)
  local copies, waits for them, and re-layouts  12.4 us (6%)
  other arithmetic  12.4 us (6%)
  starting transfers between devices  11.3 us (5%)
  matrix products  6.78 us (3%)
  waiting for transfers between devices  2.27 us (1%)
    all_to_all x2, blocking collectives, stacked_from(): lax.all_to_all(jnp.stack([tiles] * lax.axis_size(axes[k])), axes[k], 0, 0)  77 us
    psum x2, blocking collectives, by_axis(): return functools.reduce(lax.psum, axes, value)  57.7 us
    all_to_all x2, blocking collectives, copy_for_each(): return lax.all_to_all(copies, axis, split_axis=0, concat_axis=0, tiled=True)  17.7 us
    ppermute x2, starting transfers between devices, passed_along(): return lax.ppermute(block, axis, route)  6.42 us
    unnamed x17, local copies, waits for them, and re-layouts  5.09 us
    reduce_sum x2, other arithmetic, on_device(): jnp.sum(conv_grad * padded[k:k + rows], axis=0)  4.73 us
    dot_general x1, matrix products, on_device(): lax.dot_general(columns, act, (((0,), (0,)), ((), ())), preferred_element...  4.37 us
  transfers between devices with their start and end apart: 6, of which 1 were waited for; matrix products, arithmetic and copies ran while one was open for 10% of the time, Pallas kernels for 0%

profile of v1, /device:TPU:2, one launch (start us, length us, event | category | flops | bytes accessed | tf_op | source)
XLA Modules:
  0.0 211.9 jit_solution(3735356709747553879)
XLA Ops:
  7.2 1.3 fusion.62
  8.5 3.5 %collective-permute-start = (bf16[15,256]{1,0:T(8,128)(2,1)S(1)}, bf16[15,256]{1,0:T(8,128)(2,1)S(1)}, u32[]{:S(2)}, u32[]{:S(2)}) collective-permute-start(bf16[15,256]{1,0:T(8,128)(2,1)S(1)} %get-tuple-element.109), channel_id=1, source_target_pairs={{0,8},{8,16},{16,24},{24,32},{32,40},{40,48},{48,56},{56,64},{64,7... | collective-permute-start | bytes 23048 | tf_op jit(solution)/shard_map/ppermute | solution.py:19
  12.0 1.3 collective-permute-start.1
  13.3 1.0 fusion.75
  14.3 1.0 fusion.76
  15.3 2.2 %collective-permute-done.1 = bf16[15,256]{1,0:T(8,128)(2,1)S(1)} collective-permute-done((bf16[15,256]{1,0:T(8,128)(2,1)S(1)}, bf16[15,256]{1,0:T(8,128)(2,1)S(1)}, u32[]{:S(2)}, u32[]{:S(2)}) %collective-permute-start.1) | collective-permute-done | bytes 7712 | tf_op jit(solution)/shard_map/ppermute | solution.py:21
  17.6 2.2 %fusion.72 = (f32[360]{0:T(512)S(1)}, f32[360]{0:T(512)S(1)}, f32[360,256]{1,0:T(8,128)}) fusion(f32[390,256]{1,0:T(8,128)S(1)} %maximum_convert_fusion, f32[256]{0:T(256)S(1)} %bitcast.138, f32[256]{0:T(256)S(1)} %bitcast.140, f32[256]{0:T(256)S(1)} %bitcast.82, f32[256]{0:T(256)S(1)} %bitcast.84, f32[256]{0:T(256)S(1)} %bitcast.86, f32[256]{0:T(256)S(1)} %bitcast.88, ...), kind=kLoop, calls=%fused_computation.158 | loop fusion | flops 5897520 | bytes 11831104 | tf_op jit(solution)/shard_map/reduce_sum | solution.py:99
  19.9 10.0 %all_to_all.22 = f32[8,1,720]{2,1,0:T(1,128)S(1)} all-to-all(f32[8,1,720]{2,1,0:T(1,128)S(1)} %broadcast_in_dim.4), channel_id=1, replica_groups=mesh['sp_0'=8,'sp_1'=8,'tp'=8] {'tp'}, dimensions={0} | all-to-all | bytes 46080 | tf_op jit(solution)/shard_map/all_to_all | solution.py:30
  30.0 4.4 %convolution_bitcast_fusion = f32[4096,256]{0,1:T(8,128)} fusion(bf16[360,4096]{1,0:T(8,128)(2,1)S(1)} %copy-done, f32[360,256]{1,0:T(8,128)} %get-tuple-element.104, f32[256]{0:T(256)S(1)} %copy-done.7, f32[256]{0:T(256)S(1)} %copy-done.6, f32[360]{0:T(512)S(1)} %get-tuple-element.145, f32[360]{0:T(512)S(1)} %get-tuple-element.144), kind=kOutput, calls=%fused_computation | convolution fusion | flops 755804160 | bytes 7516992 | tf_op jit(solution)/shard_map/dot_general | solution.py:143
  35.2 22.6 %all_to_all.23 = bf16[8,1,256,64]{2,3,1,0:T(8,128)(2,1)S(1)} all-to-all(bf16[8,1,256,64]{2,3,1,0:T(8,128)(2,1)S(1)} %stack.102), channel_id=1, replica_groups=mesh['sp_0'=8,'sp_1'=8,'tp'=8] {'sp_0'}, dimensions={0} | all-to-all | bytes 524288 | tf_op jit(solution)/shard_map/all_to_all | solution.py:57
  58.1 54.4 %all_to_all.24 = bf16[8,8,256,64]{2,3,1,0:T(8,128)(2,1)S(1)} all-to-all(bf16[8,8,256,64]{2,3,1,0:T(8,128)(2,1)S(1)} %stack.103), channel_id=1, replica_groups=mesh['sp_0'=8,'sp_1'=8,'tp'=8] {'sp_1'}, dimensions={0} | all-to-all | bytes 4194304 | tf_op jit(solution)/shard_map/all_to_all | solution.py:57
  113.4 2.4 %multiply_reduce_fusion = (f32[256]{0:T(256)}, f32[360]{0:T(512)S(1)}, f32[360]{0:T(512)S(1)}, f32[256]{0:T(256)}, f32[360,256]{1,0:T(8,128)}) fusion(f32[360,256]{1,0:T(8,128)S(1)} %copy-done.1, f32[360]{0:T(512)S(1)} %get-tuple-element.145, f32[360]{0:T(512)S(1)} %get-tuple-element.144, f32[256]{0:T(256)S(1)} %copy-done.6, f32[256]{0:T(256)S(1)} %copy-done.7, ...), kind=kOutput, calls=%fused_computation.102 | convolution fusion | flops 756724480 | bytes 5793408 | tf_op jit(solution)/shard_map/dot_general | solution.py:108
  115.9 7.7 %all_to_all.25 = f32[8,1,720]{2,1,0:T(1,128)S(1)} all-to-all(f32[8,1,720]{2,1,0:T(1,128)S(1)} %broadcast_in_dim.5), channel_id=1, replica_groups=mesh['sp_0'=8,'sp_1'=8,'tp'=8] {'tp'}, dimensions={0} | all-to-all | bytes 46080 | tf_op jit(solution)/shard_map/all_to_all | solution.py:30
  123.8 2.6 %multiply_reduce_fusion.1 = (f32[256]{0:T(256)S(1)}, f32[256]{0:T(256)}, f32[256]{0:T(256)}, f32[256]{0:T(256)}, f32[256]{0:T(256)}, /*index=5*/f32[256]{0:T(256...) fusion(f32[390,256]{1,0:T(8,128)S(1)} %maximum_convert_fusion, ...), kind=kLoop, calls=%fused_computation.103 | loop fusion | flops 4050432 | bytes 7766656 | tf_op jit(solution)/shard_map/reduce_sum | solution.py:131
  127.1 1.2 fusion.55
  129.7 1.3 collective-permute-start.3
  131.0 5.1 %collective-permute-start.2 = (f32[15,256]{1,0:T(8,128)}, f32[15,256]{1,0:T(8,128)}, u32[]{:S(2)}, u32[]{:S(2)}) collective-permute-start(f32[15,256]{1,0:T(8,128)} %get-tuple-element.108), channel_id=1, source_target_pairs={{0,8},{8,16},{16,24},{24,32},{32,40},{40,48},{48,56},{56,64},{64,7... | collective-permute-start | bytes 46088 | tf_op jit(solution)/shard_map/ppermute | solution.py:72
  136.1 2.0 copy.24
  138.2 2.2 %multiply_reduce_fusion.19 = (f32[256]{0:T(256)}, f32[256]{0:T(256)}, f32[256]{0:T(256)}, f32[256]{0:T(256)}, f32[256]{0:T(256)}, /*index=5*/f32[256]{0:T(256)},...) fusion(f32[360,256]{1,0:T(8,128)} %copy-done.2, ...), kind=kLoop, calls=%fused_computation.121 | loop fusion | flops 2392832 | bytes 5174272 | tf_op jit(solution)/shard_map/reduce_sum | solution.py:131
  140.4 2.9 %stack.135 = f32[31,256]{1,0:T(8,128)S(1)} concatenate(f32[1,256]{1,0:T(1,128)} %bitcast.172, f32[1,256]{1,0:T(1,128)} %bitcast.171, f32[1,256]{1,0:T(1,128)} %bitcast.170, f32[1,256]{1,0:T(1,128)} %bitcast.169, f32[1,256]{1,0:T(1,128)} %bitcast.168, f32[1,256]{1,0:T(1,128)} %bitcast.167, f32[1,256]{1,0:T(1,128)} %bitcast.166, f32[1,256]{1,0:T(1,128)} %bitcast.165, ...), dimensions={0} | concatenate | bytes 63488 | tf_op jit(solution)/shard_map/stack | solution.py:131
  143.3 27.9 %all-reduce.2 = (f32[31,256]{1,0:T(8,128)S(1)}, f32[256]{0:T(256)S(1)}, f32[256]{0:T(256)S(1)}) all-reduce(f32[31,256]{1,0:T(8,128)S(1)} %stack.135, f32[256]{0:T(256)} %get-tuple-element.91, f32[256]{0:T(256)} %get-tuple-element.94), channel_id=1, replica_groups=mesh['sp_0'=8,'sp_1'=8,'tp'=8] {'sp_0'}, use_global_device_ids=true, to_apply=%region_37.38 | all-reduce | flops 8448 | bytes 67584 | tf_op jit(solution)/shard_map/psum | solution.py:76
  171.2 29.8 %all-reduce.1 = (f32[31,256]{1,0:T(8,128)}, f32[256]{0:T(256)}, f32[256]{0:T(256)}) all-reduce(f32[31,256]{1,0:T(8,128)S(1)} %get-tuple-element.100, f32[256]{0:T(256)S(1)} %get-tuple-element.101, f32[256]{0:T(256)S(1)} %get-tuple-element.102), channel_id=1, replica_groups=mesh['sp_0'=8,'sp_1'=8,'tp'=8] {'sp_1'}, use_global_device_ids=true, to_apply=%region_38.39 | all-reduce | flops 8448 | bytes 67584 | tf_op jit(solution)/shard_map/psum | solution.py:76
  201.0 1.0 slice.544
  203.2 1.8 fusion.65
  (43 shorter events, 5.8 us)
Async XLA Ops:
  7.2 22.9 %copy-start = (bf16[360,4096]{1,0:T(8,128)(2,1)S(1)}, bf16[360,4096]{1,0:T(8,128)(2,1)}, u32[]{:S(2)}) copy-start(bf16[360,4096]{1,0:T(8,128)(2,1)} %param.17) | copy-start | bytes 8847364
  7.2 129.0 %reduce-scatter.5.cloned.1.call-start = ((), (), s32[]{:S(2)}) async-start(), calls=%async_computation.6 | async-start | bytes 4718592 | tf_op jit(solution)/shard_map/reduce_scatter | solution.py:81
  8.5 6.8 %collective-permute-start = (bf16[15,256]{1,0:T(8,128)(2,1)S(1)}, bf16[15,256]{1,0:T(8,128)(2,1)S(1)}, u32[]{:S(2)}, u32[]{:S(2)}) collective-permute-start(bf16[15,256]{1,0:T(8,128)(2,1)S(1)} %get-tuple-element.109), channel_id=1, source_target_pairs={{0,8},{8,16},{16,24},{24,32},{32,40},{40,48},{48,56},{56,64},{64,7... | collective-permute-start | bytes 23048 | tf_op jit(solution)/shard_map/ppermute | solution.py:19
  12.0 5.5 %collective-permute-start.1 = (bf16[15,256]{1,0:T(8,128)(2,1)S(1)}, bf16[15,256]{1,0:T(8,128)(2,1)S(1)}, u32[]{:S(2)}, u32[]{:S(2)}) collective-permute-start(bf16[15,256]{1,0:T(8,128)(2,1)S(1)} %get-tuple-element.110), channel_id=1, source_target_pairs={{8,0},{16,8},{24,16},{32,24},{40,32},{48,40},{56,48},{64,56},{72,6... | collective-permute-start | bytes 23048 | tf_op jit(solution)/shard_map/ppermute | solution.py:21
  17.6 12.4 %copy-start.6 = (f32[256]{0:T(256)S(1)}, f32[256]{0:T(256)}, u32[]{:S(2)}) copy-start(f32[256]{0:T(256)} %param.14) | copy-start | bytes 3076
  17.6 12.4 %copy-start.7 = (f32[256]{0:T(256)S(1)}, f32[256]{0:T(256)}, u32[]{:S(2)}) copy-start(f32[256]{0:T(256)} %param.15) | copy-start | bytes 3076
  34.4 0.8 copy-start.5
  34.4 170.6 %reduce-scatter.7.cloned.1.call-start = ((), (), s32[]{:S(2)}) async-start(), calls=%async_computation.7 | async-start | bytes 589824
  112.4 1.0 copy-start.1
  126.4 0.7 copy-start.2
  128.3 0.8 copy-start.3
  129.7 73.3 %collective-permute-start.3 = (f32[15,256]{1,0:T(8,128)}, f32[15,256]{1,0:T(8,128)S(1)}, u32[]{:S(2)}, u32[]{:S(2)}) collective-permute-start(f32[15,256]{1,0:T(8,128)} %get-tuple-element.107), channel_id=1, source_target_pairs={{8,0},{16,8},{24,16},{32,24},{40,32},{48,40},{56,48},{64,56},{72,6... | collective-permute-start | bytes 46088 | tf_op jit(solution)/shard_map/ppermute | solution.py:72
  131.0 71.0 %collective-permute-start.2 = (f32[15,256]{1,0:T(8,128)}, f32[15,256]{1,0:T(8,128)}, u32[]{:S(2)}, u32[]{:S(2)}) collective-permute-start(f32[15,256]{1,0:T(8,128)} %get-tuple-element.108), channel_id=1, source_target_pairs={{0,8},{8,16},{16,24},{24,32},{32,40},{40,48},{48,56},{56,64},{64,7... | collective-permute-start | bytes 46088 | tf_op jit(solution)/shard_map/ppermute | solution.py:72
  138.2 65.0 %copy-start.4 = (bf16[360,256]{1,0:T(8,128)(2,1)S(1)}, bf16[360,256]{1,0:T(8,128)(2,1)}, u32[]{:S(2)}) copy-start(bf16[360,256]{1,0:T(8,128)(2,1)} %param.11) | copy-start | bytes 552964
Sparse Core Ops, SparseCore 0:
  34.5 61.9 reduce-scatter.4
  138.3 33.3 reduce-scatter.6
